TPU v7x, 512 devices: a whole 4x4x16 slice. The times are simulated.
512 devices in a mesh: sp: 32 (over z, core), tp: 16 (over y, x).
Axes of the slice: x: 4, y: 4, z: 16, core: 2. Of those that a mesh axis runs over, the one named last changes fastest.
Arguments:
- residual_in: bfloat16 [8192, 2048], P('sp'), may hold values from -3 to 3
- mix_gain: float32 [2048], replicated, may hold values from 0.1 to 1.9
- pool_weight: bfloat16 [512, 2048], P(None, 'tp'), may hold values from -0.5 to 0.5
- pool_scale: float32 [2048], P('tp'), may hold values from 0.1 to 1.9
- ffn_gain: float32 [2048], replicated, may hold values from 0.1 to 1.9
- route_ids: int32 [8192, 2], P('sp'), may hold values from 0 to 31, all different within a row; in each aligned block of 16 rows (0 to 15, 16 to 31, ...) at most 2 rows name the same one
- route_weights: float32 [8192, 2], P('sp'), may hold values from 0.1 to 1
- gate_weight: bfloat16 [32, 2048, 3584], P('sp', None, 'tp'), may hold values from -0.125 to 0.125
- up_weight: bfloat16 [32, 2048, 3584], P('sp', None, 'tp'), may hold values from -0.125 to 0.125
- down_weight: bfloat16 [32, 3584, 2048], P('sp', 'tp'), may hold values from -0.09375 to 0.09375
Outputs:
- layer_out: bfloat16 [8192, 2048], P('sp')
Inputs may be any that keep to these rules, and one draw needn't show every extreme that they name: `route_ids`: each row names 2 different experts; in each aligned block of 16 rows no expert is named by more than 2 rows, and some block has an expert named by exactly 2 rows.
All inputs are finite; a program needn't handle non-finite values.
Results may differ from a plain program's by a relative error of at most 0.0074.
Values may be sent and summed in bfloat16 or wider, within the bound.
No kernel may reach another device: no remote copies, remote signals or barrier semaphores. Data moves between devices by JAX's collectives and lax.ppermute only.
A program may use at most 64 MiB of HBM per device.

v0:
```python
import jax
import jax.numpy as jnp
from jax import lax
from jax.sharding import Mesh
from jax.sharding import PartitionSpec as P

GROUPS = 4
SPAN = 16
TOP_K = 2
SP = ("sp_0", "sp_1")
EPS = 1e-06


def from_behind(value, axis, steps):
    count = lax.axis_size(axis)
    first, last = (max(0, -steps), min(count, count - steps))
    return lax.ppermute(value, axis, [(source, source + steps) for source in range(first, last)])


def split_up(shard, dim, size):
    before, after = (shard.shape[:dim], shard.shape[dim + 1 :])
    return jnp.moveaxis(shard.reshape(*before, size, -1, *after), dim, 0)


def sent_and_summed(shard, axis, dim):
    size = lax.axis_size(axis)
    blocks = lax.all_to_all(split_up(shard, dim, size), axis, 0, 0, tiled=True)
    return jnp.sum(blocks.astype(jnp.float32), axis=0)


def in_order(blocks, dim):
    dims = list(blocks.shape[1:])
    dims[dim] *= blocks.shape[0]
    return jnp.moveaxis(blocks, 0, dim).reshape(dims)


def exchange_in_order(blocks, axes, order):
    dims = [lax.axis_size(a) for a in axes]
    blocks = blocks.reshape(*dims, *blocks.shape[1:])
    for k in order:
        blocks = lax.all_to_all(blocks, axes[k], split_axis=k, concat_axis=k, tiled=True)
    return blocks.reshape(-1, *blocks.shape[len(axes) :])


def core_and_chips(shard, groups, order, split_dim, concat_dim):
    size = lax.axis_size(groups[0]) * lax.axis_size(groups[1])
    blocks = split_up(shard, split_dim, size)
    return in_order(exchange_in_order(blocks, groups, order), concat_dim)


def copy_for_each(shard, axis):
    size = lax.axis_size(axis)
    return lax.all_to_all(
        jnp.broadcast_to(shard[None], (size, *shard.shape)), axis, 0, 0, tiled=True
    )


def gather_directly(shard, axis, dim):
    blocks = copy_for_each(shard, axis)
    return in_order(blocks, dim)


def rms_scale(values, gain):
    return values * lax.rsqrt(jnp.mean(values * values, axis=-1, keepdims=True) + EPS) * gain


def slot_table(chosen_ids, experts, capacity):
    flat_ids = chosen_ids.reshape(-1)
    matches = (flat_ids[:, None] == jnp.arange(experts, dtype=jnp.int32)[None, :]).astype(jnp.int32)
    before = jnp.cumsum(matches, axis=0) - matches
    slot_of = jnp.sum(before * matches, axis=1)
    target = flat_ids * capacity + slot_of
    return (target[:, None] == jnp.arange(experts * capacity, dtype=jnp.int32)[None, :]).astype(
        jnp.float32
    )


def shards(
    residual_in,
    mix_gain,
    pool_weight,
    pool_scale,
    ffn_gain,
    route_ids,
    route_weights,
    gate_weight,
    up_weight,
    down_weight,
):
    tp_count = lax.axis_size("tp")
    sp_count = lax.axis_size(SP)
    tp_index = lax.axis_index("tp")
    tok_count, width = residual_in.shape
    group_width = width // GROUPS
    col_count = pool_weight.shape[1]
    row_count = tok_count // tp_count
    capacity = 2 * TOP_K * row_count // sp_count
    group_index = tp_index * col_count // group_width
    window = jnp.power(2, group_index + 1)
    stream = residual_in.astype(jnp.float32)
    inverse = lax.rsqrt(jnp.mean(stream * stream, axis=-1, keepdims=True) + EPS)
    stream_group = lax.dynamic_slice_in_dim(stream, group_index * group_width, group_width, 1)
    gain_group = lax.dynamic_slice_in_dim(mix_gain, group_index * group_width, group_width, 0)
    normed_group = (stream_group * inverse * gain_group).astype(jnp.bfloat16)
    rim_rows = from_behind(normed_group[tok_count - SPAN :], SP, 1)
    extended = jnp.concatenate([rim_rows, normed_group], axis=0).astype(jnp.float32)
    window_sum = jnp.zeros((tok_count, group_width), jnp.float32)
    for offset in range(SPAN):
        window_sum = window_sum + jnp.where(
            offset < window, extended[SPAN - offset : SPAN - offset + tok_count], 0.0
        )
    position = lax.axis_index(SP) * tok_count + jnp.arange(tok_count, dtype=jnp.int32)
    divisor = jnp.minimum(position + 1, window).astype(jnp.float32)
    pooled = (window_sum / divisor[:, None] - extended[SPAN:]).astype(jnp.bfloat16)
    mixed = (jnp.dot(pooled, pool_weight, preferred_element_type=jnp.float32) * pool_scale).astype(
        jnp.bfloat16
    )
    stream_own = lax.dynamic_slice_in_dim(stream, tp_index * row_count, row_count, 0)
    mixed_own = lax.all_to_all(mixed, "tp", split_axis=0, concat_axis=1, tiled=True)
    after_own = (stream_own + mixed_own.astype(jnp.float32)).astype(jnp.bfloat16)
    normed_own = rms_scale(after_own.astype(jnp.float32), ffn_gain).astype(jnp.bfloat16)
    ids_own = lax.dynamic_slice_in_dim(route_ids, tp_index * row_count, row_count, 0)
    table_own = slot_table(ids_own, sp_count, capacity)
    repeated = jnp.repeat(normed_own, TOP_K, axis=0)
    outgoing = lax.dot_general(
        table_own.astype(jnp.bfloat16),
        repeated,
        (((0,), (0,)), ((), ())),
        preferred_element_type=jnp.float32,
    )
    outgoing = outgoing.astype(jnp.bfloat16).reshape(sp_count, capacity, width)
    arrived = lax.all_to_all(outgoing, SP, split_axis=0, concat_axis=0, tiled=True)
    piece = lax.all_gather(arrived, "tp", axis=0, tiled=True)
    flat_rows = piece.reshape(-1, width)
    gate_part = jnp.dot(flat_rows, gate_weight[0], preferred_element_type=jnp.float32)
    up_part = jnp.dot(flat_rows, up_weight[0], preferred_element_type=jnp.float32)
    hidden = (jax.nn.silu(gate_part) * up_part).astype(jnp.bfloat16)
    hidden_all = hidden.reshape(piece.shape[0], piece.shape[1], hidden.shape[1])
    hidden_flat = hidden_all.reshape(-1, hidden_all.shape[-1])
    term = jnp.dot(hidden_flat, down_weight[0], preferred_element_type=jnp.float32)
    summed = sent_and_summed(
        term.astype(jnp.bfloat16).astype(jnp.float32).astype(jnp.bfloat16), "tp", 0
    )
    expert_out = summed.astype(jnp.bfloat16).reshape(sp_count, capacity, width)
    returned_rows = core_and_chips(expert_out, ("sp_0", "sp_1"), (1, 0), 0, 0)
    weights_own = lax.dynamic_slice_in_dim(route_weights, tp_index * row_count, row_count, 0)
    weight_table = jnp.einsum(
        "rk,rkc->rc", weights_own, table_own.reshape(row_count, TOP_K, sp_count * capacity)
    )
    expert_mix = jnp.dot(
        weight_table,
        returned_rows.reshape(-1, width).astype(jnp.float32),
        precision=lax.Precision.HIGHEST,
    )
    out_own = (after_own.astype(jnp.float32) + expert_mix).astype(jnp.bfloat16)
    return gather_directly(out_own, "tp", 0)


def solution(mesh):
    torus = Mesh(mesh.devices.reshape(16, 2, mesh.shape["tp"]), ("sp_0", "sp_1", "tp"))
    return jax.shard_map(
        shards,
        mesh=torus,
        in_specs=(
            P(SP, None),
            P(),
            P(None, "tp"),
            P("tp"),
            P(),
            P(SP, None),
            P(SP, None),
            P(SP, None, "tp"),
            P(SP, None, "tp"),
            P(SP, "tp", None),
        ),
        out_specs=P(SP, None),
        check_vma=False,
    )
```

profile of v0, /device:TPU:32, one launch (start us, length us, event | category | flops | bytes accessed | tf_op | source)
XLA Modules:
  0.0 268.7 jit_solution(1426922073096499499)
XLA Ops:
  6.5 0.0 copy-start
  6.5 0.0 copy-start.2
  6.5 0.0 copy-start.6
  6.5 0.0 copy-start.5
  6.5 1.6 multiply_reduce_fusion
  8.1 1.5 convert_element_type.67
  9.6 0.8 dynamic_slice.17
  10.4 0.1 multiply_convert_fusion
  10.5 1.9 collective-permute-start
  12.5 0.0 copy-done.2
  12.5 0.1 constant_dynamic-slice_fusion
  12.6 0.1 copy.24
  12.7 0.1 eq.35
  12.8 0.1 fusion.40
  12.8 0.1 reduce_window_sum.11
  12.9 0.2 select_reduce_fusion
  13.1 2.5 collective-permute-done
  15.6 0.1 maximum_convert_fusion
  15.7 0.0 copy-done.6
  15.7 0.0 copy-done.5
  15.7 0.0 copy-start.1
  15.7 2.0 fusion.2
  17.7 7.0 %all-to-all-start = ((bf16[16,16,128]{2,1,0:T(8,128)(2,1)}), bf16[16,16,128]{2,1,0:T(8,128)(2,1)S(1)}, u32[]{:S(2)}, u32[]{:S(2)}) async-start(bf16[16,16,128]{2,1,0:T(8,128)(2,1)} %bitcast), calls=%async_computation | async-start | bytes 131072 | tf_op jit(solution)/shard_map/all_to_all | solution.py:119
  24.8 0.0 all-gather.2.cloned.1.call-start
  24.8 7.6 %all-to-all-done = bf16[16,16,128]{2,1,0:T(8,128)(2,1)S(1)} async-done(((bf16[16,16,128]{2,1,0:T(8,128)(2,1)}), bf16[16,16,128]{2,1,0:T(8,128)(2,1)S(1)}, u32[]{:S(2)}, u32[]{:S(2)}) %all-to-all-start) | async-done | bytes 65568 | tf_op jit(solution)/shard_map/all_to_all | solution.py:119
  32.4 0.1 fusion.33
  32.6 0.0 copy-done.1
  32.6 0.1 fusion.35
  32.7 0.1 broadcast_in_dim.38
  32.8 0.1 reshape.67
  32.8 0.3 convolution_convert_fusion.1
  33.2 0.2 reshape.68
  33.3 37.4 %all_to_all.38 = bf16[32,2,2048]{2,1,0:T(2,128)(2,1)} all-to-all(bf16[32,2,2048]{2,1,0:T(2,128)(2,1)S(1)} %reshape.68), channel_id=1, replica_groups=mesh['sp_0'=16,'sp_1'=2,'tp'=16] {'sp_0','sp_1'}, dimensions={0} | all-to-all | bytes 524288 | tf_op jit(solution)/shard_map/all_to_all | solution.py:132
  70.8 0.0 all-gather.2.cloned.1.call-update
  70.8 0.0 copy-start.3
  70.8 56.0 %all-gather.2.cloned.1.call-done = bf16[512,2,2048]{2,1,0:T(2,128)(2,1)} async-done(((bf16[32,2,2048]{2,1,0:T(2,128)(2,1)}), bf16[512,2,2048]{2,1,0:T(2,128)(2,1)}) %all-gather.2.cloned.1.call-update) | async-done | bytes 4194320 | tf_op jit(solution)/shard_map/all_gather | solution.py:133
  126.8 7.2 %reshape.69 = bf16[1024,2048]{1,0:T(8,128)(2,1)} reshape(bf16[512,2,2048]{2,1,0:T(2,128)(2,1)} %all-gather.2.cloned.1.call-done) | data formatting | bytes 8388608 | tf_op jit(solution)/shard_map/reshape | solution.py:134
  134.0 0.0 copy-done.3
  134.0 0.0 copy-start.4
  134.0 4.6 %fusion.6 = f32[1024,224]{0,1:T(8,128)} fusion(bf16[1024,2048]{1,0:T(8,128)(2,1)} %reshape.69, bf16[1,2048,224]{1,2,0:T(8,128)(2,1)S(1)} %copy-done.3), kind=kOutput, calls=%fused_computation.11 | convolution fusion | flops 939524096 | bytes 6029312 | tf_op jit(solution)/shard_map/dot_general | solution.py:135
  138.6 0.0 copy-done
  138.6 0.0 copy-done.4
  138.6 7.0 %convolution_convert_fusion = bf16[1024,2048]{1,0:T(8,128)(2,1)} fusion(bf16[1024,2048]{1,0:T(8,128)(2,1)} %reshape.69, bf16[1,224,2048]{2,1,0:T(8,128)(2,1)S(1)} %copy-done, bf16[1,2048,224]{1,2,0:T(8,128)(2,1)S(1)} %copy-done.4, f32[1024,224]{0,1:T(8,128)} %fusion.6), kind=kOutput, calls=%fused_computation | convolution fusion | flops 1882521600 | bytes 11141120 | tf_op jit(solution)/shard_map/dot_general | solution.py:140
  145.6 56.0 %all_to_all.39 = bf16[16,64,2048]{2,1,0:T(8,128)(2,1)} all-to-all(bf16[16,64,2048]{2,1,0:T(8,128)(2,1)} %bitcast.35), channel_id=1, replica_groups=mesh['sp_0'=16,'sp_1'=2,'tp'=16] {'tp'}, dimensions={0} | all-to-all | bytes 8388608 | tf_op jit(solution)/shard_map/all_to_all | solution.py:27
  201.7 3.0 %reduce_sum.45 = bf16[64,2048]{1,0:T(8,128)(2,1)S(1)} reduce(bf16[16,64,2048]{2,1,0:T(8,128)(2,1)} %all_to_all.39, bf16[]{:T(256)} %constant.97.clone.1), dimensions={0}, to_apply=%region_4.5 | reduce | flops 1966080 | bytes 4456450 | tf_op jit(solution)/shard_map/reduce_sum | solution.py:28
  204.6 0.2 reshape_reshape_reshape.6
  204.8 0.2 copy.20
  205.0 3.9 %all_to_all.40 = bf16[16,2,1,2,2048]{4,3,0,2,1:T(2,128)(2,1)S(1)} all-to-all(bf16[16,2,1,2,2048]{4,3,0,2,1:T(2,128)(2,1)S(1)} %copy.20), channel_id=1, replica_groups=mesh['sp_0'=16,'sp_1'=2,'tp'=16] {'sp_1'}, dimensions={1} | all-to-all | bytes 524288 | tf_op jit(solution)/shard_map/all_to_all | solution.py:41
  209.0 1.0 copy.21
  209.9 12.7 %all-to-all-start.4 = ((bf16[16,2,1,2,2048]{4,3,1,2,0:T(2,128)(2,1)}), bf16[16,2,1,2,2048]{4,3,1,2,0:T(2,128)(2,1)S(1)}, u32[]{:S(2)}, u32[]{:S(2)}) async-start(bf16[16,2,1,2,2048]{4,3,1,2,0:T(2,128)(2,1)} %copy.21), calls=%async_computation.4 | async-start | bytes 524288 | tf_op jit(solution)/shard_map/all_to_all | solution.py:41
  222.6 0.1 reduce_sum.43
  222.7 0.8 dynamic-slice_bitcast_fusion
  223.4 0.1 copy.22
  223.5 0.2 fusion.37
  223.7 17.2 %all-to-all-done.4 = bf16[16,2,1,2,2048]{4,3,1,2,0:T(2,128)(2,1)S(1)} async-done(((bf16[16,2,1,2,2048]{4,3,1,2,0:T(2,128)(2,1)}), bf16[16,2,1,2,2048]{4,3,1,2,0:T(2,128)(2,1)S(1)}, u32[]{:S(2)}, u32[]{:S(2)}) %all-to-all-start.4) | async-done | bytes 262176 | tf_op jit(solution)/shard_map/all_to_all | solution.py:41
  241.0 0.1 reshape_reshape_reshape.7
  241.1 0.2 fusion
  241.3 0.1 broadcast_in_dim.39
  241.4 19.5 %all_to_all.41 = bf16[16,16,2048]{2,1,0:T(8,128)(2,1)S(1)} all-to-all(bf16[16,16,2048]{2,1,0:T(8,128)(2,1)S(1)} %broadcast_in_dim.39), channel_id=1, replica_groups=mesh['sp_0'=16,'sp_1'=2,'tp'=16] {'tp'}, dimensions={0} | all-to-all | bytes 2097152 | tf_op jit(solution)/shard_map/all_to_all | solution.py:53
  260.9 1.0 copy.29
  (6 shorter events, 0.0 us)
Async XLA Ops:
  6.5 132.1 %copy-start = (bf16[1,224,2048]{2,1,0:T(8,128)(2,1)S(1)}, bf16[1,224,2048]{2,1,0:T(8,128)(2,1)}, u32[]{:S(2)}) copy-start(bf16[1,224,2048]{2,1,0:T(8,128)(2,1)} %param.19) | copy-start | bytes 2752516
  6.5 6.0 %copy-start.2 = (s32[256,2]{0,1:T(2,128)S(1)}, s32[256,2]{0,1:T(2,128)}, u32[]{:S(2)}) copy-start(s32[256,2]{0,1:T(2,128)} %param.15) | copy-start | bytes 6148
  6.5 9.1 %copy-start.6 = (f32[128]{0:T(128)S(1)}, f32[128]{0:T(128)}, u32[]{:S(2)}) copy-start(f32[128]{0:T(128)} %param.13) | copy-start | bytes 1540
  6.5 9.1 %copy-start.5 = (bf16[512,128]{1,0:T(8,128)(2,1)S(1)}, bf16[512,128]{1,0:T(8,128)(2,1)}, u32[]{:S(2)}) copy-start(bf16[512,128]{1,0:T(8,128)(2,1)} %param.12) | copy-start | bytes 393220
  10.5 5.1 %collective-permute-start = (bf16[16,512]{1,0:T(8,128)(2,1)S(1)}, bf16[16,512]{1,0:T(8,128)(2,1)S(1)}, u32[]{:S(2)}, u32[]{:S(2)}) collective-permute-start(bf16[16,512]{1,0:T(8,128)(2,1)S(1)} %slice.69), channel_id=1, source_target_pairs={{0,16},{16,32},{32,48},{48,64},{64,80},{80,96},{96,112},{112,128},... | collective-permute-start | bytes 49160 | tf_op jit(solution)/shard_map/ppermute | solution.py:17
  15.7 16.9 %copy-start.1 = (f32[2048]{0:T(1024)S(1)}, f32[2048]{0:T(1024)}, u32[]{:S(2)}) copy-start(f32[2048]{0:T(1024)} %param.14) | copy-start | bytes 24580
  17.7 14.7 %all-to-all-start = ((bf16[16,16,128]{2,1,0:T(8,128)(2,1)}), bf16[16,16,128]{2,1,0:T(8,128)(2,1)S(1)}, u32[]{:S(2)}, u32[]{:S(2)}) async-start(bf16[16,16,128]{2,1,0:T(8,128)(2,1)} %bitcast), calls=%async_computation | async-start | bytes 131072 | tf_op jit(solution)/shard_map/all_to_all | solution.py:119
  24.8 102.0 %all-gather.2.cloned.1.call-start = ((), (), s32[]{:S(2)}) async-start(), calls=%async_computation.6 | async-start | bytes 4456448 | tf_op jit(solution)/shard_map/all_gather | solution.py:133
  70.8 63.2 %copy-start.3 = (bf16[1,2048,224]{1,2,0:T(8,128)(2,1)S(1)}, bf16[1,2048,224]{1,2,0:T(8,128)(2,1)}, u32[]{:S(2)}) copy-start(bf16[1,2048,224]{1,2,0:T(8,128)(2,1)} %param.17) | copy-start | bytes 2752516
  134.0 4.6 %copy-start.4 = (bf16[1,2048,224]{1,2,0:T(8,128)(2,1)S(1)}, bf16[1,2048,224]{1,2,0:T(8,128)(2,1)}, u32[]{:S(2)}) copy-start(bf16[1,2048,224]{1,2,0:T(8,128)(2,1)} %param.18) | copy-start | bytes 2752516
  209.9 31.0 %all-to-all-start.4 = ((bf16[16,2,1,2,2048]{4,3,1,2,0:T(2,128)(2,1)}), bf16[16,2,1,2,2048]{4,3,1,2,0:T(2,128)(2,1)S(1)}, u32[]{:S(2)}, u32[]{:S(2)}) async-start(bf16[16,2,1,2,2048]{4,3,1,2,0:T(2,128)(2,1)} %copy.21), calls=%async_computation.4 | async-start | bytes 524288 | tf_op jit(solution)/shard_map/all_to_all | solution.py:41
Sparse Core Ops, SparseCore 0:
  70.9 55.8 all-gather.1
where the time goes:
time: 269 us
  blocking collectives  117 us (43%)
  waiting for transfers between devices  83.3 us (31%)
  starting transfers between devices  21.7 us (8%)
  matrix products  14.4 us (5%)
  between operations  13.7 us (5%)
  local copies, waits for them, and re-layouts  12 us (4%)
  other arithmetic  6.75 us (3%)
    all_to_all x1, blocking collectives, sent_and_summed(): blocks = lax.all_to_all(split_up(shard, dim, size), axis, 0, 0, tiled=True)  56 us
    all_gather x1, waiting for transfers between devices, shards(): piece = lax.all_gather(arrived, 'tp', axis=0, tiled=True)  56 us
    all_to_all x1, blocking collectives, shards(): lax.all_to_all(outgoing, SP, split_axis=0, concat_axis=0, tiled=True)  37.4 us
    all_to_all x1, blocking collectives, copy_for_each(): lax.all_to_all(jnp.broadcast_to(shard[None], (size, *shard.shape)), axis,...  19.5 us
    all_to_all x1, waiting for transfers between devices, exchange_in_order(): lax.all_to_all(blocks, axes[k], split_axis=k, concat_axis=k, tiled=True)  17.2 us
    all_to_all x1, starting transfers between devices, exchange_in_order(): lax.all_to_all(blocks, axes[k], split_axis=k, concat_axis=k, tiled=True)  12.7 us
    all_to_all x1, waiting for transfers between devices, shards(): lax.all_to_all(mixed, 'tp', split_axis=0, concat_axis=1, tiled=True)  7.6 us
    reshape x1, local copies, waits for them, and re-layouts, shards(): flat_rows = piece.reshape(-1, width)  7.21 us
  transfers between devices with their start and end apart: 4, of which 4 were waited for; matrix products, arithmetic and copies ran while one was open for 1% of the time, Pallas kernels for 0%

commit v1 on v0

--- a/solution.py
+++ b/solution.py
@@ -116,7 +116,9 @@
         jnp.bfloat16
     )
     stream_own = lax.dynamic_slice_in_dim(stream, tp_index * row_count, row_count, 0)
-    mixed_own = lax.all_to_all(mixed, "tp", split_axis=0, concat_axis=1, tiled=True)
+    parts = jnp.split(mixed, lax.axis_size("tp"), axis=0)
+    received = lax.all_to_all(jnp.stack(parts), "tp", 0, 0)
+    mixed_own = jnp.concatenate(received, axis=1)
     after_own = (stream_own + mixed_own.astype(jnp.float32)).astype(jnp.bfloat16)
     normed_own = rms_scale(after_own.astype(jnp.float32), ffn_gain).astype(jnp.bfloat16)
     ids_own = lax.dynamic_slice_in_dim(route_ids, tp_index * row_count, row_count, 0)

time: 269 us -> 278 us (1.033)
  local copies, waits for them, and re-layouts: 12 us -> 21.5 us
    unnamed x16 -> x31, local copies, waits for them, and re-layouts: 1.09 us -> 9.99 us
where the time goes in v1:
time: 278 us
  blocking collectives  117 us (42%)
  waiting for transfers between devices  83.3 us (30%)
  starting transfers between devices  21.7 us (8%)
  local copies, waits for them, and re-layouts  21.5 us (8%)
  matrix products  13.7 us (5%)
  between operations  13.7 us (5%)
  other arithmetic  6.75 us (2%)
    all_to_all x1, blocking collectives, sent_and_summed(): blocks = lax.all_to_all(split_up(shard, dim, size), axis, 0, 0, tiled=True)  56.1 us
    all_gather x1, waiting for transfers between devices, shards(): piece = lax.all_gather(arrived, 'tp', axis=0, tiled=True)  56 us
    all_to_all x1, blocking collectives, shards(): lax.all_to_all(outgoing, SP, split_axis=0, concat_axis=0, tiled=True)  37.4 us
    all_to_all x1, blocking collectives, copy_for_each(): lax.all_to_all(jnp.broadcast_to(shard[None], (size, *shard.shape)), axis,...  19.5 us
    all_to_all x1, waiting for transfers between devices, exchange_in_order(): lax.all_to_all(blocks, axes[k], split_axis=k, concat_axis=k, tiled=True)  17.2 us
    all_to_all x1, starting transfers between devices, exchange_in_order(): lax.all_to_all(blocks, axes[k], split_axis=k, concat_axis=k, tiled=True)  12.7 us
    unnamed x31, local copies, waits for them, and re-layouts  9.99 us
    all_to_all x1, waiting for transfers between devices, shards(): received = lax.all_to_all(jnp.stack(parts), 'tp', 0, 0)  7.61 us
  transfers between devices with their start and end apart: 4, of which 4 were waited for; matrix products, arithmetic and copies ran while one was open for 1% of the time, Pallas kernels for 0%

profile of v1, /device:TPU:32, one launch (start us, length us, event | category | flops | bytes accessed | tf_op | source)
XLA Modules:
  0.0 277.6 jit_solution(8813035531677727605)
XLA Ops:
  6.5 1.6 multiply_reduce_fusion
  8.1 1.5 convert_element_type.67
  9.6 0.8 dynamic_slice.17
  10.4 0.1 multiply_convert_fusion
  10.5 1.9 collective-permute-start
  12.5 0.1 constant_dynamic-slice_fusion
  12.6 0.1 copy.23
  12.7 0.1 eq.35
  12.8 0.1 fusion.40
  12.8 0.1 reduce_window_sum.11
  12.9 0.2 select_reduce_fusion
  13.1 2.5 collective-permute-done
  15.6 0.1 maximum_convert_fusion
  15.7 0.0 copy-start.1
  15.7 1.4 fusion.2
  17.1 0.6 constant_dynamic-update-slice_fusion.15
  17.7 0.6 constant_dynamic-update-slice_fusion.14
  18.3 0.6 constant_dynamic-update-slice_fusion.13
  18.9 0.6 constant_dynamic-update-slice_fusion.12
  19.5 0.6 constant_dynamic-update-slice_fusion.11
  20.1 0.6 constant_dynamic-update-slice_fusion.10
  20.7 0.6 constant_dynamic-update-slice_fusion.9
  21.3 0.6 constant_dynamic-update-slice_fusion.8
  21.8 0.6 constant_dynamic-update-slice_fusion.7
  22.4 0.6 constant_dynamic-update-slice_fusion.6
  23.0 0.6 constant_dynamic-update-slice_fusion.5
  23.6 0.6 constant_dynamic-update-slice_fusion.4
  24.2 0.6 constant_dynamic-update-slice_fusion.3
  24.8 0.6 constant_dynamic-update-slice_fusion.2
  25.4 0.6 constant_dynamic-update-slice_fusion.1
  26.0 0.6 constant_dynamic-update-slice_fusion
  26.6 7.0 %all-to-all-start = ((bf16[16,16,128]{2,1,0:T(8,128)(2,1)}), bf16[16,16,128]{2,1,0:T(8,128)(2,1)S(1)}, u32[]{:S(2)}, u32[]{:S(2)}) async-start(bf16[16,16,128]{2,1,0:T(8,128)(2,1)} %constant_dynamic-update-slice_fusion), calls=%async_computation | async-start | bytes 131072 | tf_op jit(solution)/shard_map/all_to_all | solution.py:120
  33.6 0.0 all-gather.2.cloned.1.call-start
  33.7 7.6 %all-to-all-done = bf16[16,16,128]{2,1,0:T(8,128)(2,1)S(1)} async-done(((bf16[16,16,128]{2,1,0:T(8,128)(2,1)}), bf16[16,16,128]{2,1,0:T(8,128)(2,1)S(1)}, u32[]{:S(2)}, u32[]{:S(2)}) %all-to-all-start) | async-done | bytes 65568 | tf_op jit(solution)/shard_map/all_to_all | solution.py:120
  41.3 0.1 fusion.33
  41.5 0.1 fusion.35
  41.5 0.1 broadcast_in_dim.38
  41.6 0.1 reshape.66
  41.7 0.3 convolution_convert_fusion.1
  42.0 0.2 reshape.67
  42.2 37.4 %all_to_all.30 = bf16[32,2,2048]{2,1,0:T(2,128)(2,1)} all-to-all(bf16[32,2,2048]{2,1,0:T(2,128)(2,1)S(1)} %reshape.67), channel_id=1, replica_groups=mesh['sp_0'=16,'sp_1'=2,'tp'=16] {'sp_0','sp_1'}, dimensions={0} | all-to-all | bytes 524288 | tf_op jit(solution)/shard_map/all_to_all | solution.py:134
  79.6 0.0 all-gather.2.cloned.1.call-update
  79.7 0.0 copy-start.3
  79.7 56.0 %all-gather.2.cloned.1.call-done = bf16[512,2,2048]{2,1,0:T(2,128)(2,1)} async-done(((bf16[32,2,2048]{2,1,0:T(2,128)(2,1)}), bf16[512,2,2048]{2,1,0:T(2,128)(2,1)}) %all-gather.2.cloned.1.call-update) | async-done | bytes 4194320 | tf_op jit(solution)/shard_map/all_gather | solution.py:135
  135.7 7.2 %reshape.68 = bf16[1024,2048]{1,0:T(8,128)(2,1)} reshape(bf16[512,2,2048]{2,1,0:T(2,128)(2,1)} %all-gather.2.cloned.1.call-done) | data formatting | bytes 8388608 | tf_op jit(solution)/shard_map/reshape | solution.py:136
  142.9 4.6 %fusion.6 = f32[1024,224]{0,1:T(8,128)} fusion(bf16[1024,2048]{1,0:T(8,128)(2,1)} %reshape.68, bf16[1,2048,224]{1,2,0:T(8,128)(2,1)S(1)} %copy-done.3), kind=kOutput, calls=%fused_computation.11 | convolution fusion | flops 939524096 | bytes 6029312 | tf_op jit(solution)/shard_map/dot_general | solution.py:137
  147.5 7.0 %convolution_convert_fusion = bf16[1024,2048]{1,0:T(8,128)(2,1)} fusion(bf16[1024,2048]{1,0:T(8,128)(2,1)} %reshape.68, bf16[1,224,2048]{2,1,0:T(8,128)(2,1)S(1)} %copy-done, bf16[1,2048,224]{1,2,0:T(8,128)(2,1)S(1)} %copy-done.4, f32[1024,224]{0,1:T(8,128)} %fusion.6), kind=kOutput, calls=%fused_computation | convolution fusion | flops 1882521600 | bytes 11141120 | tf_op jit(solution)/shard_map/dot_general | solution.py:142
  154.4 56.1 %all_to_all.31 = bf16[16,64,2048]{2,1,0:T(8,128)(2,1)} all-to-all(bf16[16,64,2048]{2,1,0:T(8,128)(2,1)} %bitcast.98), channel_id=1, replica_groups=mesh['sp_0'=16,'sp_1'=2,'tp'=16] {'tp'}, dimensions={0} | all-to-all | bytes 8388608 | tf_op jit(solution)/shard_map/all_to_all | solution.py:27
  210.5 3.0 %reduce_sum.45 = bf16[64,2048]{1,0:T(8,128)(2,1)S(1)} reduce(bf16[16,64,2048]{2,1,0:T(8,128)(2,1)} %all_to_all.31, bf16[]{:T(256)} %constant.97.clone.1), dimensions={0}, to_apply=%region_4.5 | reduce | flops 1966080 | bytes 4456450 | tf_op jit(solution)/shard_map/reduce_sum | solution.py:28
  213.5 0.2 reshape_reshape_reshape.6
  213.7 0.2 copy.19
  213.9 3.9 %all_to_all.32 = bf16[16,2,1,2,2048]{4,3,0,2,1:T(2,128)(2,1)S(1)} all-to-all(bf16[16,2,1,2,2048]{4,3,0,2,1:T(2,128)(2,1)S(1)} %copy.19), channel_id=1, replica_groups=mesh['sp_0'=16,'sp_1'=2,'tp'=16] {'sp_1'}, dimensions={1} | all-to-all | bytes 524288 | tf_op jit(solution)/shard_map/all_to_all | solution.py:41
  217.8 1.0 copy.20
  218.8 12.7 %all-to-all-start.4 = ((bf16[16,2,1,2,2048]{4,3,1,2,0:T(2,128)(2,1)}), bf16[16,2,1,2,2048]{4,3,1,2,0:T(2,128)(2,1)S(1)}, u32[]{:S(2)}, u32[]{:S(2)}) async-start(bf16[16,2,1,2,2048]{4,3,1,2,0:T(2,128)(2,1)} %copy.20), calls=%async_computation.4 | async-start | bytes 524288 | tf_op jit(solution)/shard_map/all_to_all | solution.py:41
  231.4 0.1 reduce_sum.43
  231.5 0.8 dynamic-slice_bitcast_fusion
  232.3 0.1 copy.21
  232.4 0.2 fusion.37
  232.6 17.2 %all-to-all-done.4 = bf16[16,2,1,2,2048]{4,3,1,2,0:T(2,128)(2,1)S(1)} async-done(((bf16[16,2,1,2,2048]{4,3,1,2,0:T(2,128)(2,1)}), bf16[16,2,1,2,2048]{4,3,1,2,0:T(2,128)(2,1)S(1)}, u32[]{:S(2)}, u32[]{:S(2)}) %all-to-all-start.4) | async-done | bytes 262176 | tf_op jit(solution)/shard_map/all_to_all | solution.py:41
  249.8 0.1 reshape_reshape_reshape.7
  249.9 0.2 fusion
  250.1 0.1 broadcast_in_dim.39
  250.3 19.5 %all_to_all.33 = bf16[16,16,2048]{2,1,0:T(8,128)(2,1)S(1)} all-to-all(bf16[16,16,2048]{2,1,0:T(8,128)(2,1)S(1)} %broadcast_in_dim.39), channel_id=1, replica_groups=mesh['sp_0'=16,'sp_1'=2,'tp'=16] {'tp'}, dimensions={0} | all-to-all | bytes 2097152 | tf_op jit(solution)/shard_map/all_to_all | solution.py:53
  269.8 1.0 copy.43
  (18 shorter events, 0.1 us)
Async XLA Ops:
  6.5 140.9 %copy-start = (bf16[1,224,2048]{2,1,0:T(8,128)(2,1)S(1)}, bf16[1,224,2048]{2,1,0:T(8,128)(2,1)}, u32[]{:S(2)}) copy-start(bf16[1,224,2048]{2,1,0:T(8,128)(2,1)} %param.19) | copy-start | bytes 2752516
  6.5 6.0 %copy-start.2 = (s32[256,2]{0,1:T(2,128)S(1)}, s32[256,2]{0,1:T(2,128)}, u32[]{:S(2)}) copy-start(s32[256,2]{0,1:T(2,128)} %param.15) | copy-start | bytes 6148
  6.5 9.1 %copy-start.6 = (f32[128]{0:T(128)S(1)}, f32[128]{0:T(128)}, u32[]{:S(2)}) copy-start(f32[128]{0:T(128)} %param.13) | copy-start | bytes 1540
  6.5 9.1 %copy-start.5 = (bf16[512,128]{1,0:T(8,128)(2,1)S(1)}, bf16[512,128]{1,0:T(8,128)(2,1)}, u32[]{:S(2)}) copy-start(bf16[512,128]{1,0:T(8,128)(2,1)} %param.12) | copy-start | bytes 393220
  10.5 5.1 %collective-permute-start = (bf16[16,512]{1,0:T(8,128)(2,1)S(1)}, bf16[16,512]{1,0:T(8,128)(2,1)S(1)}, u32[]{:S(2)}, u32[]{:S(2)}) collective-permute-start(bf16[16,512]{1,0:T(8,128)(2,1)S(1)} %slice.69), channel_id=1, source_target_pairs={{0,16},{16,32},{32,48},{48,64},{64,80},{80,96},{96,112},{112,128},... | collective-permute-start | bytes 49160 | tf_op jit(solution)/shard_map/ppermute | solution.py:17
  15.7 25.8 %copy-start.1 = (f32[2048]{0:T(1024)S(1)}, f32[2048]{0:T(1024)}, u32[]{:S(2)}) copy-start(f32[2048]{0:T(1024)} %param.14) | copy-start | bytes 24580
  26.6 14.7 %all-to-all-start = ((bf16[16,16,128]{2,1,0:T(8,128)(2,1)}), bf16[16,16,128]{2,1,0:T(8,128)(2,1)S(1)}, u32[]{:S(2)}, u32[]{:S(2)}) async-start(bf16[16,16,128]{2,1,0:T(8,128)(2,1)} %constant_dynamic-update-slice_fusion), calls=%async_computation | async-start | bytes 131072 | tf_op jit(solution)/shard_map/all_to_all | solution.py:120
  33.6 102.0 %all-gather.2.cloned.1.call-start = ((), (), s32[]{:S(2)}) async-start(), calls=%async_computation.6 | async-start | bytes 4456448 | tf_op jit(solution)/shard_map/all_gather | solution.py:135
  79.7 63.2 %copy-start.3 = (bf16[1,2048,224]{1,2,0:T(8,128)(2,1)S(1)}, bf16[1,2048,224]{1,2,0:T(8,128)(2,1)}, u32[]{:S(2)}) copy-start(bf16[1,2048,224]{1,2,0:T(8,128)(2,1)} %param.17) | copy-start | bytes 2752516
  142.9 4.6 %copy-start.4 = (bf16[1,2048,224]{1,2,0:T(8,128)(2,1)S(1)}, bf16[1,2048,224]{1,2,0:T(8,128)(2,1)}, u32[]{:S(2)}) copy-start(bf16[1,2048,224]{1,2,0:T(8,128)(2,1)} %param.18) | copy-start | bytes 2752516
  218.8 31.0 %all-to-all-start.4 = ((bf16[16,2,1,2,2048]{4,3,1,2,0:T(2,128)(2,1)}), bf16[16,2,1,2,2048]{4,3,1,2,0:T(2,128)(2,1)S(1)}, u32[]{:S(2)}, u32[]{:S(2)}) async-start(bf16[16,2,1,2,2048]{4,3,1,2,0:T(2,128)(2,1)} %copy.20), calls=%async_computation.4 | async-start | bytes 524288 | tf_op jit(solution)/shard_map/all_to_all | solution.py:41
Sparse Core Ops, SparseCore 0:
  79.8 55.8 all-gather.1
